TPU v7x, 32 devices: a whole 2x2x4 slice. The times are simulated.
32 devices in a mesh: ep: 8 (over z, y), tp: 4 (over x, core).
Axes of the slice: x: 2, y: 2, z: 4, core: 2. Of those that a mesh axis runs over, the one named last changes fastest.
Arguments:
- mixer_in: bfloat16 [4096, 4096], P(('ep', 'tp')), may hold values from -6 to 6
- mixer_gain: float32 [4096], replicated, may hold values from 0.1 to 1.9
- group_weight: bfloat16 [4, 1024, 1024], P('tp'), may hold values from -0.1875 to 0.1875
- group_scale: float32 [4, 1024], P('tp'), may hold values from 0.1 to 1.9
- expert_in: bfloat16 [4096, 4096], P(('ep', 'tp')), may hold values from -6 to 6
- expert_gain: float32 [4096], replicated, may hold values from 0.1 to 1.9
- routes: int32 [4096, 2], P('ep'), may hold values from 0 to 7, all different within a row; in each aligned block of 128 rows (0 to 127, 128 to 255, ...) at most 48 rows name the same one
- route_weight: float32 [4096, 2], P('ep'), may hold values from 0.2 to 1
- gate_weight: bfloat16 [8, 4096, 1024], P('ep', None, 'tp'), may hold values from -0.25 to 0.25
- up_weight: bfloat16 [8, 4096, 1024], P('ep', None, 'tp'), may hold values from -0.25 to 0.25
- down_weight: bfloat16 [8, 1024, 4096], P('ep', 'tp'), may hold values from -0.02734375 to 0.02734375
Outputs:
- mixed: bfloat16 [4096, 4096], P('ep', 'tp')
- expert_out: bfloat16 [4096, 4096], P(('ep', 'tp'))
Inputs may be any that keep to these rules, and one draw needn't show every extreme that they name: `routes`: each row names 2 different experts; within the rows of one device (aligned blocks of 128 rows) no expert is named more than 48 times, and that count is reached.
All inputs are finite; a program needn't handle non-finite values.
Results may differ from a plain program's by a relative error of at most 0.012.
Values may be sent and summed in bfloat16 or wider, within the bound.
A program may use at most 128 MiB of HBM per device.

v0:
```python
import jax
import jax.numpy as jnp
from jax import lax
from jax.sharding import PartitionSpec as P

WMAX = 16
CHUNKS = 3
epsilon = 1e-06
clamp_limit = 7.0
sigmoid_slope = 1.702


def from_behind(x, axis, by):
    count = lax.axis_size(axis)
    pairs = [(i, i + by) for i in range(count) if 0 <= i + by < count]
    return lax.ppermute(x, axis, pairs)


def rms_norm(values, gain):
    widened = values.astype(jnp.float32)
    scaled = widened * lax.rsqrt(jnp.mean(widened * widened, axis=-1, keepdims=True) + epsilon)
    return (scaled * gain).astype(jnp.bfloat16)


def clamped_unit(gate_part, up_part):
    gate_part = jnp.minimum(gate_part, clamp_limit)
    up_part = jnp.clip(up_part, -clamp_limit, clamp_limit)
    return ((up_part + 1.0) * gate_part * jax.nn.sigmoid(sigmoid_slope * gate_part)).astype(
        jnp.bfloat16
    )


def slot_ids(block_routes, experts, capacity):
    onehot = (
        block_routes[:, :, None] == jnp.arange(experts, dtype=jnp.int32)[None, None, :]
    ).astype(jnp.float32)
    per_token = jnp.sum(onehot, axis=1)
    count = block_routes.shape[0]
    before = (
        jnp.arange(count, dtype=jnp.int32)[:, None] > jnp.arange(count, dtype=jnp.int32)[None, :]
    ).astype(jnp.bfloat16)
    earlier = jnp.dot(before, per_token.astype(jnp.bfloat16), preferred_element_type=jnp.float32)
    rank = jnp.sum(onehot * earlier[:, None, :], axis=2).astype(jnp.int32)
    return (block_routes, rank)


def mixer_rows(mixer_in, mixer_gain):
    normed = rms_norm(mixer_in, mixer_gain)
    shard_rows = lax.all_to_all(normed, "tp", split_axis=1, concat_axis=0, tiled=True)
    length = shard_rows.shape[0]
    return (shard_rows, from_behind(shard_rows[length - WMAX :], "ep", 1))


def mixer(shard_rows, before, group_weight, group_scale):
    length = shard_rows.shape[0]
    total = jnp.concatenate([before, shard_rows], axis=0).astype(jnp.float32)
    values = total[WMAX:]
    tp_index = lax.axis_index("tp")
    window = 2 << tp_index
    position = lax.axis_index("ep") * length + jnp.arange(length, dtype=jnp.int32)
    picked = jnp.zeros_like(values)
    reach = 1
    for level in range(lax.axis_size("tp")):
        total = total[reach:] + total[:-reach]
        reach = 2 * reach
        picked = jnp.where(tp_index == level, total[total.shape[0] - length :], picked)
    counts = jnp.minimum(position + 1, window).astype(jnp.float32)[:, None]
    pooled = (picked / counts - values).astype(jnp.bfloat16)
    return (
        jnp.dot(pooled, group_weight[0], preferred_element_type=jnp.float32) * group_scale[0]
    ).astype(jnp.bfloat16)


def shards(
    mixer_in,
    mixer_gain,
    group_weight,
    group_scale,
    expert_in,
    expert_gain,
    routes,
    route_weight,
    gate_weight,
    up_weight,
    down_weight,
):
    shard_rows, before = mixer_rows(mixer_in, mixer_gain)
    expert_in, shard_rows, before = lax.optimization_barrier((expert_in, shard_rows, before))
    mixed = mixer(shard_rows, before, group_weight, group_scale)
    expert_norm = rms_norm(expert_in, expert_gain)
    tok_count, width = expert_in.shape
    top = routes.shape[1]
    experts = lax.axis_size("ep")
    capacity = max(2, 3 * tok_count * top // (2 * experts))
    chunks = CHUNKS if capacity % CHUNKS == 0 else 1
    part = capacity // chunks
    tp_index = lax.axis_index("tp")
    own_routes = lax.dynamic_slice_in_dim(routes, tp_index * tok_count, tok_count, 0)
    own_weight = lax.dynamic_slice_in_dim(route_weight, tp_index * tok_count, tok_count, 0)
    gate_local = gate_weight[0]
    up_local = up_weight[0]
    down_full = lax.all_gather(down_weight[0], "tp", axis=0, tiled=True)
    expert_of, rank = slot_ids(own_routes, experts, capacity)
    expert_sum = jnp.zeros((tok_count, width), jnp.float32)
    pieces = []
    picks = []
    for chunk in range(chunks):
        inside = (rank >= chunk * part) & (rank < (chunk + 1) * part)
        slot = jnp.where(inside, expert_of * part + rank - chunk * part, -1)
        match = slot[:, :, None] == jnp.arange(experts * part, dtype=jnp.int32)[None, None, :]
        picks.append(match)
        pick = jnp.any(match, axis=1).astype(jnp.bfloat16)
        outgoing = lax.dot_general(
            pick, expert_norm, (((0,), (0,)), ((), ())), preferred_element_type=jnp.float32
        ).astype(jnp.bfloat16)
        if chunk > 0:
            outgoing, arrived = lax.optimization_barrier((outgoing, arrived))
        arrived = lax.all_to_all(outgoing, "ep", split_axis=0, concat_axis=0, tiled=True)
        if chunk == 1:
            arrived, down_full = lax.optimization_barrier((arrived, down_full))
        pieces.append(lax.all_gather(arrived, "tp", axis=0, tiled=True))
    for chunk in range(chunks):
        piece = pieces[chunk]
        if chunk > 0:
            piece, result = lax.optimization_barrier((piece, result))
        hidden = clamped_unit(
            jnp.dot(piece, gate_local, preferred_element_type=jnp.float32),
            jnp.dot(piece, up_local, preferred_element_type=jnp.float32),
        )
        hidden = lax.all_to_all(hidden, "tp", split_axis=0, concat_axis=1, tiled=True)
        result = jnp.dot(hidden, down_full, preferred_element_type=jnp.float32).astype(jnp.bfloat16)
        returned = lax.all_to_all(result, "ep", split_axis=0, concat_axis=0, tiled=True)
        weights = jnp.sum(jnp.where(picks[chunk], own_weight[:, :, None], 0.0), axis=1)
        high = weights.astype(jnp.bfloat16)
        low = (weights - high.astype(jnp.float32)).astype(jnp.bfloat16)
        expert_sum = (
            expert_sum
            + jnp.dot(high, returned, preferred_element_type=jnp.float32)
            + jnp.dot(low, returned, preferred_element_type=jnp.float32)
        )
    return (mixed, expert_sum.astype(jnp.bfloat16))


def solution(mesh):
    in_specs = (
        P(("ep", "tp"), None),
        P(),
        P("tp", None, None),
        P("tp", None),
        P(("ep", "tp"), None),
        P(),
        P("ep", None),
        P("ep", None),
        P("ep", None, "tp"),
        P("ep", None, "tp"),
        P("ep", "tp", None),
    )
    out_specs = (P("ep", "tp"), P(("ep", "tp"), None))
    return jax.shard_map(shards, mesh=mesh, in_specs=in_specs, out_specs=out_specs, check_vma=False)
```

profile of v0, /device:TPU:0, one launch (start us, length us, event | category | flops | bytes accessed | tf_op | source)
XLA Modules:
  0.0 288.4 jit_solution(611450616829126164)
XLA Ops:
  7.2 0.7 all-gather.12.cloned.1.call-update
  7.9 1.6 copy.39
  9.5 0.6 fusion.1
  10.1 1.5 fusion.3
  11.6 4.4 %all-to-all-start = ((bf16[128,4,1024]{0,2,1:T(8,128)(2,1)}), bf16[128,4,1024]{0,2,1:T(8,128)(2,1)}, u32[]{:S(2)}, u32[]{:S(2)}) async-start(bf16[128,4,1024]{0,2,1:T(8,128)(2,1)} %bitcast.115), calls=%async_computation | async-start | bytes 2097152 | tf_op jit(solution)/shard_map/all_to_all | solution.py:49
  16.1 0.1 fusion.86
  16.3 22.9 %all-to-all-done = bf16[128,4,1024]{0,2,1:T(8,128)(2,1)} async-done(((bf16[128,4,1024]{0,2,1:T(8,128)(2,1)}), bf16[128,4,1024]{0,2,1:T(8,128)(2,1)}, u32[]{:S(2)}, u32[]{:S(2)}) %all-to-all-start) | async-done | bytes 1048608 | tf_op jit(solution)/shard_map/all_to_all | solution.py:49
  39.2 2.3 copy.40
  41.5 0.8 slice.56
  42.3 5.4 %collective-permute-start = (bf16[16,1024]{1,0:T(8,128)(2,1)S(1)}, bf16[16,1024]{1,0:T(8,128)(2,1)}, u32[]{:S(2)}, u32[]{:S(2)}) collective-permute-start(bf16[16,1024]{1,0:T(8,128)(2,1)S(1)} %slice.56), channel_id=1, source_target_pairs={{0,4},{4,8},{8,12},{12,16},{16,20},{20,24},{24,28},{1,5},{5,9},{9,... | collective-permute-start | bytes 98312 | tf_op jit(solution)/shard_map/ppermute | solution.py:16
  47.8 0.8 collective-permute-done
  48.6 0.3 fusion.4
  48.9 0.5 convolution_convert_fusion.5
  49.4 30.4 %all_to_all.148 = bf16[8,16,4096]{2,1,0:T(8,128)(2,1)} all-to-all(bf16[8,16,4096]{2,1,0:T(8,128)(2,1)S(1)} %bitcast.117), channel_id=1, replica_groups=mesh['ep'=8,'tp'=4] {'ep'}, dimensions={0} | all-to-all | bytes 2097152 | tf_op jit(solution)/shard_map/all_to_all | solution.py:118
  80.0 0.5 convolution_convert_fusion.4
  80.5 28.0 %all_to_all.149 = bf16[8,16,4096]{2,1,0:T(8,128)(2,1)} all-to-all(bf16[8,16,4096]{2,1,0:T(8,128)(2,1)S(1)} %bitcast.118), channel_id=1, replica_groups=mesh['ep'=8,'tp'=4] {'ep'}, dimensions={0} | all-to-all | bytes 2097152 | tf_op jit(solution)/shard_map/all_to_all | solution.py:118
  108.6 0.5 convolution_convert_fusion.1
  109.1 28.9 %all_to_all.150 = bf16[8,16,4096]{2,1,0:T(8,128)(2,1)} all-to-all(bf16[8,16,4096]{2,1,0:T(8,128)(2,1)S(1)} %bitcast.116), channel_id=1, replica_groups=mesh['ep'=8,'tp'=4] {'ep'}, dimensions={0} | all-to-all | bytes 2097152 | tf_op jit(solution)/shard_map/all_to_all | solution.py:118
  138.1 4.3 %fusion.28 = f32[512,256]{1,0:T(8,128)S(1)} fusion(bf16[512,4096]{1,0:T(8,128)(2,1)} %all-gather.6.cloned.1.call-done, bf16[1,4096,256]{2,1,0:T(8,128)(2,1)} %param.19), kind=kOutput, calls=%fused_computation.48 | convolution fusion | flops 1073872896 | bytes 6815744 | tf_op jit(solution)/shard_map/dot_general | solution.py:127
  142.4 0.5 copy-done.12
  142.9 1.3 fusion.73
  144.2 0.2 copy.41
  144.3 8.8 %all_to_all.151 = bf16[4,128,256]{1,2,0:T(8,128)(2,1)S(1)} all-to-all(bf16[4,128,256]{1,2,0:T(8,128)(2,1)S(1)} %copy.41), channel_id=1, replica_groups=mesh['ep'=8,'tp'=4] {'tp'}, dimensions={0} | all-to-all | bytes 524288 | tf_op jit(solution)/shard_map/all_to_all | solution.py:130
  153.2 5.6 %convolution_convert_fusion.3 = bf16[128,4096]{1,0:T(8,128)(2,1)} fusion(bf16[128,1024]{0,1:T(8,128)(2,1)S(1)} %bitcast.127, bf16[1024,4096]{1,0:T(8,128)(2,1)} %bitcast.106), kind=kOutput, calls=%fused_computation.9 | convolution fusion | flops 1074266112 | bytes 9699328 | tf_op jit(solution)/shard_map/dot_general | solution.py:131
  158.8 4.9 %fusion.31 = f32[512,256]{1,0:T(8,128)S(1)} fusion(bf16[512,4096]{1,0:T(8,128)(2,1)} %all-gather.8.cloned.1.call-done, bf16[1,4096,256]{2,1,0:T(8,128)(2,1)} %param.19), kind=kOutput, calls=%fused_computation.49 | convolution fusion | flops 1073872896 | bytes 6815744 | tf_op jit(solution)/shard_map/dot_general | solution.py:127
  163.7 0.5 copy-done.11
  164.2 0.7 copy-done.13
  164.9 1.3 fusion.76
  166.2 0.2 copy.42
  166.4 11.6 %all_to_all.152 = bf16[4,128,256]{1,2,0:T(8,128)(2,1)S(1)} all-to-all(bf16[4,128,256]{1,2,0:T(8,128)(2,1)S(1)} %copy.42), channel_id=1, replica_groups=mesh['ep'=8,'tp'=4] {'tp'}, dimensions={0} | all-to-all | bytes 524288 | tf_op jit(solution)/shard_map/all_to_all | solution.py:130
  178.0 4.0 %all-to-all-start.4 = ((bf16[8,16,4096]{2,1,0:T(8,128)(2,1)}), bf16[8,16,4096]{2,1,0:T(8,128)(2,1)S(1)}, u32[]{:S(2)}, u32[]{:S(2)}) async-start(bf16[8,16,4096]{2,1,0:T(8,128)(2,1)} %bitcast.123), calls=%async_computation.4 | async-start | bytes 2097152 | tf_op jit(solution)/shard_map/all_to_all | solution.py:132
  182.0 0.7 constant_dynamic-slice_fusion
  182.7 0.8 select_reduce_fusion
  183.5 5.7 %convolution_convert_fusion.2 = bf16[128,4096]{1,0:T(8,128)(2,1)} fusion(bf16[128,1024]{0,1:T(8,128)(2,1)S(1)} %bitcast.126, bf16[1024,4096]{1,0:T(8,128)(2,1)} %bitcast.107), kind=kOutput, calls=%fused_computation.8 | convolution fusion | flops 1074266112 | bytes 9699328 | tf_op jit(solution)/shard_map/dot_general | solution.py:131
  189.2 1.9 all-gather.10.cloned.1.call-done
  191.1 4.3 %fusion.34 = f32[512,256]{1,0:T(8,128)S(1)} fusion(bf16[512,4096]{1,0:T(8,128)(2,1)} %all-gather.10.cloned.1.call-done, bf16[1,4096,256]{2,1,0:T(8,128)(2,1)} %param.19), kind=kOutput, calls=%fused_computation.50 | convolution fusion | flops 1073872896 | bytes 6815744 | tf_op jit(solution)/shard_map/dot_general | solution.py:127
  195.4 0.5 copy-done.14
  195.8 1.3 fusion.79
  197.1 0.8 copy.43
  197.9 9.8 %all-to-all-done.4 = bf16[8,16,4096]{2,1,0:T(8,128)(2,1)S(1)} async-done(((bf16[8,16,4096]{2,1,0:T(8,128)(2,1)}), bf16[8,16,4096]{2,1,0:T(8,128)(2,1)S(1)}, u32[]{:S(2)}, u32[]{:S(2)}) %all-to-all-start.4) | async-done | bytes 1048608 | tf_op jit(solution)/shard_map/all_to_all | solution.py:132
  207.7 3.4 %all-to-all-start.8 = ((bf16[4,128,256]{1,2,0:T(8,128)(2,1)}), bf16[4,128,256]{1,2,0:T(8,128)(2,1)S(1)}, u32[]{:S(2)}, u32[]{:S(2)}) async-start(bf16[4,128,256]{1,2,0:T(8,128)(2,1)} %copy.43), calls=%async_computation.8 | async-start | bytes 524288 | tf_op jit(solution)/shard_map/all_to_all | solution.py:130
  211.2 2.9 %maximum_convert_fusion = f32[528,1024]{1,0:T(8,128)} fusion(bf16[512,1024]{1,0:T(8,128)(2,1)} %bitcast.114, bf16[16,1024]{1,0:T(8,128)(2,1)} %collective-permute-done), kind=kLoop, calls=%fused_computation.66 | loop fusion | flops 2162688 | bytes 3244032 | tf_op jit(solution)/shard_map/convert_element_type | solution.py:56
  214.1 3.0 %all-to-all-done.8 = bf16[4,128,256]{1,2,0:T(8,128)(2,1)S(1)} async-done(((bf16[4,128,256]{1,2,0:T(8,128)(2,1)}), bf16[4,128,256]{1,2,0:T(8,128)(2,1)S(1)}, u32[]{:S(2)}, u32[]{:S(2)}) %all-to-all-start.8) | async-done | bytes 262176 | tf_op jit(solution)/shard_map/all_to_all | solution.py:130
  217.1 4.2 %all-to-all-start.6 = ((bf16[8,16,4096]{2,1,0:T(8,128)(2,1)}), bf16[8,16,4096]{2,1,0:T(8,128)(2,1)}, u32[]{:S(2)}, u32[]{:S(2)}) async-start(bf16[8,16,4096]{2,1,0:T(8,128)(2,1)} %bitcast.122), calls=%async_computation.6 | async-start | bytes 2097152 | tf_op jit(solution)/shard_map/all_to_all | solution.py:132
  221.4 2.7 slice_add_fusion.2
  224.1 0.3 slice_add_fusion.1
  224.4 1.1 copy-done.1
  225.5 0.4 slice_add_fusion
  225.9 0.9 copy-done.2
  226.8 2.6 fusion.99
  229.4 0.6 copy-done.3
  230.0 1.4 slice-done.1
  231.4 2.3 convolution_convert_fusion
  233.6 13.5 %all-to-all-done.6 = bf16[8,16,4096]{2,1,0:T(8,128)(2,1)} async-done(((bf16[8,16,4096]{2,1,0:T(8,128)(2,1)}), bf16[8,16,4096]{2,1,0:T(8,128)(2,1)}, u32[]{:S(2)}, u32[]{:S(2)}) %all-to-all-start.6) | async-done | bytes 1048608 | tf_op jit(solution)/shard_map/all_to_all | solution.py:132
  247.1 4.2 %all-to-all-start.9 = ((bf16[8,16,4096]{2,1,0:T(8,128)(2,1)}), bf16[8,16,4096]{2,1,0:T(8,128)(2,1)}, u32[]{:S(2)}, u32[]{:S(2)}) async-start(bf16[8,16,4096]{2,1,0:T(8,128)(2,1)} %bitcast.124), calls=%async_computation.9 | async-start | bytes 2097152 | tf_op jit(solution)/shard_map/all_to_all | solution.py:132
  251.4 7.7 %multiply_convert_fusion = bf16[512,1024]{1,0:T(8,128)(2,1)} fusion(bf16[1,1024,1024]{2,1,0:T(8,128)(2,1)S(1)} %copy-done, f32[1024]{0:T(1024)S(1)} %bitcast.131, f32[528,1024]{1,0:T(8,128)} %maximum_convert_fusion, f32[527,1024]{1,0:T(8,128)} %copy-done.1, f32[525,1024]{1,0:T(8,128)} %copy-done.2, f32[521,1024]{1,0:T(8,128)} %copy-done.3, ...), kind=kOutput, calls=%fused_computation.47 | convolution fusion | flops 1078984704 | bytes 15734788 | tf_op jit(solution)/shard_map/dot_general | solution.py:70
  259.0 0.4 fusion.92
  259.5 0.4 convolution_add_fusion.4
  259.9 0.4 copy-done.5
  260.3 1.6 convolution_add_fusion.3
  261.9 3.0 %convolution_add_fusion.2 = f32[128,4096]{1,0:T(8,128)} fusion(f32[128,4096]{1,0:T(8,128)S(1)} %convolution_add_fusion.3, bf16[128,4096]{1,0:T(8,128)(2,1)} %bitcast.21, f32[128,128]{1,0:T(8,128)S(1)} %copy-done.5), kind=kOutput, calls=%fused_computation.2 | convolution fusion | flops 134807552 | bytes 5308416 | tf_op jit(solution)/shard_map/dot_general | solution.py:139
  264.9 12.0 %all-to-all-done.9 = bf16[8,16,4096]{2,1,0:T(8,128)(2,1)} async-done(((bf16[8,16,4096]{2,1,0:T(8,128)(2,1)}), bf16[8,16,4096]{2,1,0:T(8,128)(2,1)}, u32[]{:S(2)}, u32[]{:S(2)}) %all-to-all-start.9) | async-done | bytes 1048608 | tf_op jit(solution)/shard_map/all_to_all | solution.py:132
  276.9 2.3 convolution_add_fusion.1
  279.3 2.6 fusion
  (47 shorter events, 0.6 us)
Async XLA Ops:
  7.2 244.2 %copy-start = (bf16[1,1024,1024]{2,1,0:T(8,128)(2,1)S(1)}, bf16[1,1024,1024]{2,1,0:T(8,128)(2,1)}, u32[]{:S(2)}) copy-start(bf16[1,1024,1024]{2,1,0:T(8,128)(2,1)} %param.13) | copy-start | bytes 6291460
  7.2 101.4 %all-gather.12.cloned.1.call-start = ((), (), s32[]{:S(2)}) async-start(), calls=%async_computation.13 | async-start | bytes 10485760 | tf_op jit(solution)/shard_map/all_gather | solution.py:102
  7.9 2.2 copy-start.7
  10.1 6.0 %copy-start.8 = (s32[512,2]{0,1:T(2,128)S(1)}, s32[512,2]{0,1:T(2,128)}, u32[]{:S(2)}) copy-start(s32[512,2]{0,1:T(2,128)} %param.17) | copy-start | bytes 12292
  11.6 37.0 %copy-start.4 = (bf16[128,4096]{1,0:T(8,128)(2,1)S(1)}, bf16[128,4096]{1,0:T(8,128)(2,1)}, u32[]{:S(2)}) copy-start(bf16[128,4096]{1,0:T(8,128)(2,1)} %param.15) | copy-start | bytes 3145732
  11.6 27.6 %all-to-all-start = ((bf16[128,4,1024]{0,2,1:T(8,128)(2,1)}), bf16[128,4,1024]{0,2,1:T(8,128)(2,1)}, u32[]{:S(2)}, u32[]{:S(2)}) async-start(bf16[128,4,1024]{0,2,1:T(8,128)(2,1)} %bitcast.115), calls=%async_computation | async-start | bytes 2097152 | tf_op jit(solution)/shard_map/all_to_all | solution.py:49
  16.0 32.9 %copy-start.6 = (f32[4096]{0:T(1024)S(1)}, f32[4096]{0:T(1024)}, u32[]{:S(2)}) copy-start(f32[4096]{0:T(1024)} %param.16) | copy-start | bytes 49156
  16.0 122.0 %all-gather.6.cloned.1.call-start = ((), (), s32[]{:S(2)}) async-start(), calls=%async_computation.10 | async-start | bytes 5242880 | tf_op jit(solution)/shard_map/all_gather | solution.py:121
  42.3 6.3 %collective-permute-start = (bf16[16,1024]{1,0:T(8,128)(2,1)S(1)}, bf16[16,1024]{1,0:T(8,128)(2,1)}, u32[]{:S(2)}, u32[]{:S(2)}) collective-permute-start(bf16[16,1024]{1,0:T(8,128)(2,1)S(1)} %slice.56), channel_id=1, source_target_pairs={{0,4},{4,8},{8,12},{12,16},{16,20},{20,24},{24,28},{1,5},{5,9},{9,... | collective-permute-start | bytes 98312 | tf_op jit(solution)/shard_map/ppermute | solution.py:16
  79.9 79.0 %all-gather.8.cloned.1.call-start = ((), (), s32[]{:S(2)}) async-start(), calls=%async_computation.11 | async-start | bytes 5242880 | tf_op jit(solution)/shard_map/all_gather | solution.py:121
  108.6 82.5 %all-gather.10.cloned.1.call-start = ((), (), s32[]{:S(2)}) async-start(), calls=%async_computation.12 | async-start | bytes 5242880 | tf_op jit(solution)/shard_map/all_gather | solution.py:121
  138.1 4.3 %copy-start.10 = (bf16[512,4096]{1,0:T(8,128)(2,1)S(1)}, bf16[512,4096]{1,0:T(8,128)(2,1)}, u32[]{:S(2)}) copy-start(bf16[512,4096]{1,0:T(8,128)(2,1)} %all-gather.6.cloned.1.call-done) | copy-start | bytes 12582916
  138.1 4.8 %copy-start.12 = (bf16[1,4096,256]{2,1,0:T(8,128)(2,1)S(1)}, bf16[1,4096,256]{2,1,0:T(8,128)(2,1)}, u32[]{:S(2)}) copy-start(bf16[1,4096,256]{2,1,0:T(8,128)(2,1)} %param.20) | copy-start | bytes 6291460
  158.8 5.4 %copy-start.11 = (bf16[512,4096]{1,0:T(8,128)(2,1)S(1)}, bf16[512,4096]{1,0:T(8,128)(2,1)}, u32[]{:S(2)}) copy-start(bf16[512,4096]{1,0:T(8,128)(2,1)} %all-gather.8.cloned.1.call-done) | copy-start | bytes 12582916
  158.8 6.1 %copy-start.13 = (bf16[1,4096,256]{2,1,0:T(8,128)(2,1)S(1)}, bf16[1,4096,256]{2,1,0:T(8,128)(2,1)}, u32[]{:S(2)}) copy-start(bf16[1,4096,256]{2,1,0:T(8,128)(2,1)} %param.20) | copy-start | bytes 6291460
  178.0 29.7 %all-to-all-start.4 = ((bf16[8,16,4096]{2,1,0:T(8,128)(2,1)}), bf16[8,16,4096]{2,1,0:T(8,128)(2,1)S(1)}, u32[]{:S(2)}, u32[]{:S(2)}) async-start(bf16[8,16,4096]{2,1,0:T(8,128)(2,1)} %bitcast.123), calls=%async_computation.4 | async-start | bytes 2097152 | tf_op jit(solution)/shard_map/all_to_all | solution.py:132
  191.1 4.3 %copy-start.9 = (bf16[512,4096]{1,0:T(8,128)(2,1)S(1)}, bf16[512,4096]{1,0:T(8,128)(2,1)}, u32[]{:S(2)}) copy-start(bf16[512,4096]{1,0:T(8,128)(2,1)} %all-gather.10.cloned.1.call-done) | copy-start | bytes 12582916
  191.1 4.7 %copy-start.14 = (bf16[1,4096,256]{2,1,0:T(8,128)(2,1)S(1)}, bf16[1,4096,256]{2,1,0:T(8,128)(2,1)}, u32[]{:S(2)}) copy-start(bf16[1,4096,256]{2,1,0:T(8,128)(2,1)} %param.20) | copy-start | bytes 6291460
  207.7 9.4 %all-to-all-start.8 = ((bf16[4,128,256]{1,2,0:T(8,128)(2,1)}), bf16[4,128,256]{1,2,0:T(8,128)(2,1)S(1)}, u32[]{:S(2)}, u32[]{:S(2)}) async-start(bf16[4,128,256]{1,2,0:T(8,128)(2,1)} %copy.43), calls=%async_computation.8 | async-start | bytes 524288 | tf_op jit(solution)/shard_map/all_to_all | solution.py:130
  217.1 30.0 %all-to-all-start.6 = ((bf16[8,16,4096]{2,1,0:T(8,128)(2,1)}), bf16[8,16,4096]{2,1,0:T(8,128)(2,1)}, u32[]{:S(2)}, u32[]{:S(2)}) async-start(bf16[8,16,4096]{2,1,0:T(8,128)(2,1)} %bitcast.122), calls=%async_computation.6 | async-start | bytes 2097152 | tf_op jit(solution)/shard_map/all_to_all | solution.py:132
  224.1 1.4 copy-start.1
  224.1 5.9 %slice-start = ((s8[8388608]{0:T(1024)(128)(4,1)}), s8[4194304]{0:T(1024)(128)(4,1)S(1)}, s32[]{:S(2)}) async-start(s8[8388608]{0:T(1024)(128)(4,1)} %bitcast.108), calls=%async_computation.14 | async-start | bytes 8388608
  225.5 1.3 copy-start.2
  225.5 5.9 %slice-start.1 = ((s8[8388608]{0:T(1024)(128)(4,1)}), s8[4194304]{0:T(1024)(128)(4,1)S(1)}, s32[]{:S(2)}) async-start(s8[8388608]{0:T(1024)(128)(4,1)} %bitcast.108), calls=%async_computation.15 | async-start | bytes 8388608
  226.8 3.2 %copy-start.3 = (f32[521,1024]{1,0:T(8,128)}, f32[521,1024]{1,0:T(8,128)S(1)}, u32[]{:S(2)}) copy-start(f32[521,1024]{1,0:T(8,128)S(1)} %slice_add_fusion) | copy-start | bytes 6402052
  233.6 17.7 %copy-start.15 = (f32[1,1024]{1,0:T(1,128)S(1)}, f32[1,1024]{1,0:T(1,128)}, u32[]{:S(2)}) copy-start(f32[1,1024]{1,0:T(1,128)} %param.14) | copy-start | bytes 12292
  247.1 29.8 %all-to-all-start.9 = ((bf16[8,16,4096]{2,1,0:T(8,128)(2,1)}), bf16[8,16,4096]{2,1,0:T(8,128)(2,1)}, u32[]{:S(2)}, u32[]{:S(2)}) async-start(bf16[8,16,4096]{2,1,0:T(8,128)(2,1)} %bitcast.124), calls=%async_computation.9 | async-start | bytes 2097152 | tf_op jit(solution)/shard_map/all_to_all | solution.py:132
  259.5 0.8 copy-start.5
Sparse Core Ops, SparseCore 0:
  9.5 68.2 all-gather.11
  80.0 34.9 all-gather.5
  116.5 34.4 all-gather.7
  152.4 38.6 all-gather.9
where the time goes:
time: 289 us; the launch traced here: 288 us
  blocking collectives  108 us (37%)
  waiting for transfers between devices  64.7 us (22%)
  matrix products  50.6 us (18%)
  starting transfers between devices  25.8 us (9%)
  local copies, waits for them, and re-layouts  15.6 us (5%)
  between operations  14.1 us (5%)
  other arithmetic  9.82 us (3%)
    all_to_all x3, blocking collectives, shards(): lax.all_to_all(outgoing, 'ep', split_axis=0, concat_axis=0, tiled=True)  87.3 us
    all_to_all x3, waiting for transfers between devices, shards(): lax.all_to_all(result, 'ep', split_axis=0, concat_axis=0, tiled=True)  35.2 us
    all_to_all x1, waiting for transfers between devices, mixer_rows(): lax.all_to_all(normed, 'tp', split_axis=1, concat_axis=0, tiled=True)  22.9 us
    all_to_all x2, blocking collectives, shards(): lax.all_to_all(hidden, 'tp', split_axis=0, concat_axis=1, tiled=True)  20.5 us
    dot_general x3, matrix products, shards(): jnp.dot(hidden, down_full, preferred_element_type=jnp.float32)  13.6 us
    dot_general x3, matrix products, shards(): jnp.dot(piece, gate_local, preferred_element_type=jnp.float32)  13.4 us
    all_to_all x3, starting transfers between devices, shards(): lax.all_to_all(result, 'ep', split_axis=0, concat_axis=0, tiled=True)  12.5 us
    unnamed x37, local copies, waits for them, and re-layouts  8.1 us
  transfers between devices with their start and end apart: 10, of which 7 were waited for; matrix products, arithmetic and copies ran while one was open for 22% of the time, Pallas kernels for 0%

commit v1 on v0

--- a/solution.py
+++ b/solution.py
@@ -127,7 +127,13 @@
             jnp.dot(piece, gate_local, preferred_element_type=jnp.float32),
             jnp.dot(piece, up_local, preferred_element_type=jnp.float32),
         )
-        hidden = lax.all_to_all(hidden, "tp", split_axis=0, concat_axis=1, tiled=True)
+        recover_lines = lambda field, in_dim, dim_i: jnp.concatenate(
+            lax.all_to_all(
+                jnp.stack(jnp.split(field, lax.axis_size("tp"), axis=in_dim)), "tp", 0, 0
+            ),
+            axis=dim_i,
+        )
+        hidden = recover_lines(hidden, in_dim=0, dim_i=1)
         result = jnp.dot(hidden, down_full, preferred_element_type=jnp.float32).astype(jnp.bfloat16)
         returned = lax.all_to_all(result, "ep", split_axis=0, concat_axis=0, tiled=True)
         weights = jnp.sum(jnp.where(picks[chunk], own_weight[:, :, None], 0.0), axis=1)

time: 289 us -> 292 us (1.010)
  blocking collectives: 108 us -> 87.3 us
  waiting for transfers between devices: 64.7 us -> 75.6 us
  starting transfers between devices: 25.8 us -> 32.8 us
  matrix products: 50.6 us -> 54 us
    all_to_all x2 -> x0, blocking collectives: 20.5 us -> none  [shards(): lax.all_to_all(hidden, 'tp', split_axis=0, concat_axis=1, tiled=True)]
    all_to_all x1 -> x3, waiting for transfers between devices: 3.04 us -> 16.7 us  [shards(): lax.all_to_all(jnp.stack(jnp.split(field, lax.axis_size('tp'), axis=in_di...]
    all_to_all x1 -> x3, starting transfers between devices: 3.4 us -> 10.2 us  [shards(): lax.all_to_all(jnp.stack(jnp.split(field, lax.axis_size('tp'), axis=in_di...]
    dot_general x3, matrix products: 13.6 us -> 17 us  [shards(): jnp.dot(hidden, down_full, preferred_element_type=jnp.float32)]
  transfers between devices with their start and end apart: 10 -> 12, of which waited for: 7 -> 8; matrix products, arithmetic and copies ran while one was open for 22% -> 25% of each run, Pallas kernels for 0% -> 0%
where the time goes in v1:
time: 292 us; the launch traced here: 291 us
  blocking collectives  87.3 us (30%)
  waiting for transfers between devices  75.6 us (26%)
  matrix products  54 us (18%)
  starting transfers between devices  32.8 us (11%)
  local copies, waits for them, and re-layouts  14.7 us (5%)
  between operations  14.2 us (5%)
  other arithmetic  12.3 us (4%)
    all_to_all x3, blocking collectives, shards(): lax.all_to_all(outgoing, 'ep', split_axis=0, concat_axis=0, tiled=True)  87.3 us
    all_to_all x3, waiting for transfers between devices, shards(): lax.all_to_all(result, 'ep', split_axis=0, concat_axis=0, tiled=True)  34.4 us
    all_to_all x1, waiting for transfers between devices, mixer_rows(): lax.all_to_all(normed, 'tp', split_axis=1, concat_axis=0, tiled=True)  22.9 us
    dot_general x3, matrix products, shards(): jnp.dot(hidden, down_full, preferred_element_type=jnp.float32)  17 us
    all_to_all x3, waiting for transfers between devices, shards(): lax.all_to_all(jnp.stack(jnp.split(field, lax.axis_size('tp'), axis=in_di...  16.7 us
    dot_general x3, matrix products, shards(): jnp.dot(piece, gate_local, preferred_element_type=jnp.float32)  13.4 us
    all_to_all x3, starting transfers between devices, shards(): lax.all_to_all(result, 'ep', split_axis=0, concat_axis=0, tiled=True)  12.6 us
    all_to_all x3, starting transfers between devices, shards(): lax.all_to_all(jnp.stack(jnp.split(field, lax.axis_size('tp'), axis=in_di...  10.2 us
  transfers between devices with their start and end apart: 12, of which 8 were waited for; matrix products, arithmetic and copies ran while one was open for 25% of the time, Pallas kernels for 0%

profile of v1, /device:TPU:0, one launch (start us, length us, event | category | flops | bytes accessed | tf_op | source)
XLA Modules:
  0.0 290.8 jit_solution(7579406890513456842)
XLA Ops:
  7.2 0.7 all-gather.12.cloned.1.call-update
  7.9 1.6 copy.39
  9.5 0.6 fusion.1
  10.1 1.5 fusion.3
  11.6 4.4 %all-to-all-start = ((bf16[128,4,1024]{0,2,1:T(8,128)(2,1)}), bf16[128,4,1024]{0,2,1:T(8,128)(2,1)}, u32[]{:S(2)}, u32[]{:S(2)}) async-start(bf16[128,4,1024]{0,2,1:T(8,128)(2,1)} %bitcast.131), calls=%async_computation | async-start | bytes 2097152 | tf_op jit(solution)/shard_map/all_to_all | solution.py:49
  16.3 22.9 %all-to-all-done = bf16[128,4,1024]{0,2,1:T(8,128)(2,1)} async-done(((bf16[128,4,1024]{0,2,1:T(8,128)(2,1)}), bf16[128,4,1024]{0,2,1:T(8,128)(2,1)}, u32[]{:S(2)}, u32[]{:S(2)}) %all-to-all-start) | async-done | bytes 1048608 | tf_op jit(solution)/shard_map/all_to_all | solution.py:49
  39.2 2.3 copy.40
  41.5 0.8 slice.56
  42.3 5.4 %collective-permute-start = (bf16[16,1024]{1,0:T(8,128)(2,1)S(1)}, bf16[16,1024]{1,0:T(8,128)(2,1)}, u32[]{:S(2)}, u32[]{:S(2)}) collective-permute-start(bf16[16,1024]{1,0:T(8,128)(2,1)S(1)} %slice.56), channel_id=1, source_target_pairs={{0,4},{4,8},{8,12},{12,16},{16,20},{20,24},{24,28},{1,5},{5,9},{9,... | collective-permute-start | bytes 98312 | tf_op jit(solution)/shard_map/ppermute | solution.py:16
  47.8 0.8 collective-permute-done
  48.6 0.3 fusion.4
  48.9 0.5 convolution_convert_fusion.5
  49.5 30.4 %all_to_all.106 = bf16[8,16,4096]{2,1,0:T(8,128)(2,1)} all-to-all(bf16[8,16,4096]{2,1,0:T(8,128)(2,1)S(1)} %bitcast.133), channel_id=1, replica_groups=mesh['ep'=8,'tp'=4] {'ep'}, dimensions={0} | all-to-all | bytes 2097152 | tf_op jit(solution)/shard_map/all_to_all | solution.py:118
  80.0 0.5 convolution_convert_fusion.4
  80.6 28.0 %all_to_all.107 = bf16[8,16,4096]{2,1,0:T(8,128)(2,1)} all-to-all(bf16[8,16,4096]{2,1,0:T(8,128)(2,1)S(1)} %bitcast.134), channel_id=1, replica_groups=mesh['ep'=8,'tp'=4] {'ep'}, dimensions={0} | all-to-all | bytes 2097152 | tf_op jit(solution)/shard_map/all_to_all | solution.py:118
  108.6 0.5 convolution_convert_fusion.1
  109.2 28.9 %all_to_all.108 = bf16[8,16,4096]{2,1,0:T(8,128)(2,1)} all-to-all(bf16[8,16,4096]{2,1,0:T(8,128)(2,1)S(1)} %bitcast.132), channel_id=1, replica_groups=mesh['ep'=8,'tp'=4] {'ep'}, dimensions={0} | all-to-all | bytes 2097152 | tf_op jit(solution)/shard_map/all_to_all | solution.py:118
  138.1 4.3 %fusion.28 = f32[512,256]{1,0:T(8,128)S(1)} fusion(bf16[512,4096]{1,0:T(8,128)(2,1)} %all-gather.6.cloned.1.call-done, bf16[1,4096,256]{2,1,0:T(8,128)(2,1)} %param.19), kind=kOutput, calls=%fused_computation.48 | convolution fusion | flops 1073872896 | bytes 6815744 | tf_op jit(solution)/shard_map/dot_general | solution.py:127
  142.5 0.5 copy-done.14
  142.9 1.3 fusion.73
  144.2 0.7 pad_maximum_fusion
  145.0 3.4 %all-to-all-start.2 = ((bf16[4,128,256]{2,1,0:T(8,128)(2,1)}), bf16[4,128,256]{2,1,0:T(8,128)(2,1)S(1)}, u32[]{:S(2)}, u32[]{:S(2)}) async-start(bf16[4,128,256]{2,1,0:T(8,128)(2,1)} %pad_maximum_fusion), calls=%async_computation.2 | async-start | bytes 524288 | tf_op jit(solution)/shard_map/all_to_all | solution.py:131
  148.4 6.0 %all-to-all-done.2 = bf16[4,128,256]{2,1,0:T(8,128)(2,1)S(1)} async-done(((bf16[4,128,256]{2,1,0:T(8,128)(2,1)}), bf16[4,128,256]{2,1,0:T(8,128)(2,1)S(1)}, u32[]{:S(2)}, u32[]{:S(2)}) %all-to-all-start.2) | async-done | bytes 262176 | tf_op jit(solution)/shard_map/all_to_all | solution.py:131
  154.4 0.2 copy.41
  154.5 5.6 %convolution_convert_fusion.3 = bf16[128,4096]{1,0:T(8,128)(2,1)} fusion(bf16[128,1024]{0,1:T(8,128)(2,1)S(1)} %bitcast.142, bf16[1024,4096]{1,0:T(8,128)(2,1)} %bitcast.124), kind=kOutput, calls=%fused_computation.9 | convolution fusion | flops 1074266112 | bytes 9699328 | tf_op jit(solution)/shard_map/dot_general | solution.py:137
  160.2 4.9 %fusion.31 = f32[512,256]{1,0:T(8,128)S(1)} fusion(bf16[512,4096]{1,0:T(8,128)(2,1)} %all-gather.8.cloned.1.call-done, bf16[1,4096,256]{2,1,0:T(8,128)(2,1)} %param.19), kind=kOutput, calls=%fused_computation.49 | convolution fusion | flops 1073872896 | bytes 6815744 | tf_op jit(solution)/shard_map/dot_general | solution.py:127
  165.1 0.5 copy-done.15
  165.6 1.3 fusion.76
  166.9 0.8 pad_maximum_fusion.1
  167.6 3.4 %all-to-all-start.5 = ((bf16[4,128,256]{2,1,0:T(8,128)(2,1)}), bf16[4,128,256]{2,1,0:T(8,128)(2,1)S(1)}, u32[]{:S(2)}, u32[]{:S(2)}) async-start(bf16[4,128,256]{2,1,0:T(8,128)(2,1)} %pad_maximum_fusion.1), calls=%async_computation.5 | async-start | bytes 524288 | tf_op jit(solution)/shard_map/all_to_all | solution.py:131
  171.1 0.7 constant_dynamic-slice_fusion
  171.7 0.8 select_reduce_fusion
  172.6 7.7 %all-to-all-done.5 = bf16[4,128,256]{2,1,0:T(8,128)(2,1)S(1)} async-done(((bf16[4,128,256]{2,1,0:T(8,128)(2,1)}), bf16[4,128,256]{2,1,0:T(8,128)(2,1)S(1)}, u32[]{:S(2)}, u32[]{:S(2)}) %all-to-all-start.5) | async-done | bytes 262176 | tf_op jit(solution)/shard_map/all_to_all | solution.py:131
  180.3 4.1 %all-to-all-start.4 = ((bf16[8,16,4096]{2,1,0:T(8,128)(2,1)}), bf16[8,16,4096]{2,1,0:T(8,128)(2,1)S(1)}, u32[]{:S(2)}, u32[]{:S(2)}) async-start(bf16[8,16,4096]{2,1,0:T(8,128)(2,1)} %bitcast.138), calls=%async_computation.4 | async-start | bytes 2097152 | tf_op jit(solution)/shard_map/all_to_all | solution.py:138
  184.4 1.1 copy.42
  185.5 5.7 %convolution_convert_fusion.2 = bf16[128,4096]{1,0:T(8,128)(2,1)} fusion(bf16[128,1024]{0,1:T(8,128)(2,1)S(1)} %bitcast.143, bf16[1024,4096]{1,0:T(8,128)(2,1)} %bitcast.125), kind=kOutput, calls=%fused_computation.8 | convolution fusion | flops 1074266112 | bytes 9699328 | tf_op jit(solution)/shard_map/dot_general | solution.py:137
  191.2 4.3 %fusion.34 = f32[512,256]{1,0:T(8,128)S(1)} fusion(bf16[512,4096]{1,0:T(8,128)(2,1)} %all-gather.10.cloned.1.call-done, bf16[1,4096,256]{2,1,0:T(8,128)(2,1)} %param.19), kind=kOutput, calls=%fused_computation.50 | convolution fusion | flops 1073872896 | bytes 6815744 | tf_op jit(solution)/shard_map/dot_general | solution.py:127
  195.5 0.5 copy-done.16
  196.0 1.3 fusion.79
  197.3 0.7 pad_maximum_fusion.2
  198.0 12.1 %all-to-all-done.4 = bf16[8,16,4096]{2,1,0:T(8,128)(2,1)S(1)} async-done(((bf16[8,16,4096]{2,1,0:T(8,128)(2,1)}), bf16[8,16,4096]{2,1,0:T(8,128)(2,1)S(1)}, u32[]{:S(2)}, u32[]{:S(2)}) %all-to-all-start.4) | async-done | bytes 1048608 | tf_op jit(solution)/shard_map/all_to_all | solution.py:138
  210.1 3.4 %all-to-all-start.8 = ((bf16[4,128,256]{2,1,0:T(8,128)(2,1)}), bf16[4,128,256]{2,1,0:T(8,128)(2,1)S(1)}, u32[]{:S(2)}, u32[]{:S(2)}) async-start(bf16[4,128,256]{2,1,0:T(8,128)(2,1)} %pad_maximum_fusion.2), calls=%async_computation.8 | async-start | bytes 524288 | tf_op jit(solution)/shard_map/all_to_all | solution.py:131
  213.5 2.9 %maximum_convert_fusion = f32[528,1024]{1,0:T(8,128)} fusion(bf16[512,1024]{1,0:T(8,128)(2,1)} %bitcast.130, bf16[16,1024]{1,0:T(8,128)(2,1)} %collective-permute-done), kind=kLoop, calls=%fused_computation.66 | loop fusion | flops 2162688 | bytes 3244032 | tf_op jit(solution)/shard_map/convert_element_type | solution.py:56
  216.5 3.0 %all-to-all-done.8 = bf16[4,128,256]{2,1,0:T(8,128)(2,1)S(1)} async-done(((bf16[4,128,256]{2,1,0:T(8,128)(2,1)}), bf16[4,128,256]{2,1,0:T(8,128)(2,1)S(1)}, u32[]{:S(2)}, u32[]{:S(2)}) %all-to-all-start.8) | async-done | bytes 262176 | tf_op jit(solution)/shard_map/all_to_all | solution.py:131
  219.5 4.2 %all-to-all-start.6 = ((bf16[8,16,4096]{2,1,0:T(8,128)(2,1)}), bf16[8,16,4096]{2,1,0:T(8,128)(2,1)}, u32[]{:S(2)}, u32[]{:S(2)}) async-start(bf16[8,16,4096]{2,1,0:T(8,128)(2,1)} %bitcast.139), calls=%async_computation.6 | async-start | bytes 2097152 | tf_op jit(solution)/shard_map/all_to_all | solution.py:138
  223.7 2.8 slice_add_fusion.2
  226.6 0.4 slice_add_fusion.1
  227.0 0.9 copy-done.1
  227.9 1.3 copy-done.2
  229.3 0.4 slice_add_fusion
  229.7 2.7 fusion.99
  232.4 1.1 copy.43
  233.6 5.6 %convolution_convert_fusion = bf16[128,4096]{1,0:T(8,128)(2,1)} fusion(bf16[128,1024]{0,1:T(8,128)(2,1)S(1)} %bitcast.141, bf16[1024,4096]{1,0:T(8,128)(2,1)} %bitcast.126), kind=kOutput, calls=%fused_computation.6 | convolution fusion | flops 1074266112 | bytes 9699328 | tf_op jit(solution)/shard_map/dot_general | solution.py:137
  239.2 10.3 %all-to-all-done.6 = bf16[8,16,4096]{2,1,0:T(8,128)(2,1)} async-done(((bf16[8,16,4096]{2,1,0:T(8,128)(2,1)}), bf16[8,16,4096]{2,1,0:T(8,128)(2,1)}, u32[]{:S(2)}, u32[]{:S(2)}) %all-to-all-start.6) | async-done | bytes 1048608 | tf_op jit(solution)/shard_map/all_to_all | solution.py:138
  249.5 4.2 %all-to-all-start.9 = ((bf16[8,16,4096]{2,1,0:T(8,128)(2,1)}), bf16[8,16,4096]{2,1,0:T(8,128)(2,1)}, u32[]{:S(2)}, u32[]{:S(2)}) async-start(bf16[8,16,4096]{2,1,0:T(8,128)(2,1)} %bitcast.140), calls=%async_computation.9 | async-start | bytes 2097152 | tf_op jit(solution)/shard_map/all_to_all | solution.py:138
  253.8 7.7 %multiply_convert_fusion = bf16[512,1024]{1,0:T(8,128)(2,1)} fusion(bf16[1,1024,1024]{2,1,0:T(8,128)(2,1)S(1)} %copy-done, f32[1024]{0:T(1024)S(1)} %bitcast.147, f32[528,1024]{1,0:T(8,128)} %maximum_convert_fusion, f32[527,1024]{1,0:T(8,128)} %copy-done.1, f32[525,1024]{1,0:T(8,128)} %copy-done.2, f32[521,1024]{1,0:T(8,128)} %copy-done.3, ...), kind=kOutput, calls=%fused_computation.47 | convolution fusion | flops 1078984704 | bytes 15734788 | tf_op jit(solution)/shard_map/dot_general | solution.py:70
  261.4 0.4 fusion.92
  261.9 0.4 convolution_add_fusion.4
  262.3 0.4 copy-done.7
  262.7 1.6 convolution_add_fusion.3
  264.3 3.0 %convolution_add_fusion.2 = f32[128,4096]{1,0:T(8,128)} fusion(f32[128,4096]{1,0:T(8,128)S(1)} %convolution_add_fusion.3, bf16[128,4096]{1,0:T(8,128)(2,1)} %bitcast.27, f32[128,128]{1,0:T(8,128)S(1)} %copy-done.7), kind=kOutput, calls=%fused_computation.2 | convolution fusion | flops 134807552 | bytes 5308416 | tf_op jit(solution)/shard_map/dot_general | solution.py:145
  267.3 12.0 %all-to-all-done.9 = bf16[8,16,4096]{2,1,0:T(8,128)(2,1)} async-done(((bf16[8,16,4096]{2,1,0:T(8,128)(2,1)}), bf16[8,16,4096]{2,1,0:T(8,128)(2,1)}, u32[]{:S(2)}, u32[]{:S(2)}) %all-to-all-start.9) | async-done | bytes 1048608 | tf_op jit(solution)/shard_map/all_to_all | solution.py:138
  279.3 2.3 convolution_add_fusion.1
  281.7 2.6 fusion
  (54 shorter events, 0.8 us)
Async XLA Ops:
  7.2 246.6 %copy-start = (bf16[1,1024,1024]{2,1,0:T(8,128)(2,1)S(1)}, bf16[1,1024,1024]{2,1,0:T(8,128)(2,1)}, u32[]{:S(2)}) copy-start(bf16[1,1024,1024]{2,1,0:T(8,128)(2,1)} %param.13) | copy-start | bytes 6291460
  7.2 101.4 %all-gather.12.cloned.1.call-start = ((), (), s32[]{:S(2)}) async-start(), calls=%async_computation.13 | async-start | bytes 10485760 | tf_op jit(solution)/shard_map/all_gather | solution.py:102
  7.9 2.2 copy-start.9
  10.1 6.0 %copy-start.10 = (s32[512,2]{0,1:T(2,128)S(1)}, s32[512,2]{0,1:T(2,128)}, u32[]{:S(2)}) copy-start(s32[512,2]{0,1:T(2,128)} %param.17) | copy-start | bytes 12292
  11.6 37.0 %copy-start.4 = (bf16[128,4096]{1,0:T(8,128)(2,1)S(1)}, bf16[128,4096]{1,0:T(8,128)(2,1)}, u32[]{:S(2)}) copy-start(bf16[128,4096]{1,0:T(8,128)(2,1)} %param.15) | copy-start | bytes 3145732
  11.6 27.6 %all-to-all-start = ((bf16[128,4,1024]{0,2,1:T(8,128)(2,1)}), bf16[128,4,1024]{0,2,1:T(8,128)(2,1)}, u32[]{:S(2)}, u32[]{:S(2)}) async-start(bf16[128,4,1024]{0,2,1:T(8,128)(2,1)} %bitcast.131), calls=%async_computation | async-start | bytes 2097152 | tf_op jit(solution)/shard_map/all_to_all | solution.py:49
  16.0 32.9 %copy-start.8 = (f32[4096]{0:T(1024)S(1)}, f32[4096]{0:T(1024)}, u32[]{:S(2)}) copy-start(f32[4096]{0:T(1024)} %param.16) | copy-start | bytes 49156
  16.0 122.1 %all-gather.6.cloned.1.call-start = ((), (), s32[]{:S(2)}) async-start(), calls=%async_computation.10 | async-start | bytes 5242880 | tf_op jit(solution)/shard_map/all_gather | solution.py:121
  42.3 6.4 %collective-permute-start = (bf16[16,1024]{1,0:T(8,128)(2,1)S(1)}, bf16[16,1024]{1,0:T(8,128)(2,1)}, u32[]{:S(2)}, u32[]{:S(2)}) collective-permute-start(bf16[16,1024]{1,0:T(8,128)(2,1)S(1)} %slice.56), channel_id=1, source_target_pairs={{0,4},{4,8},{8,12},{12,16},{16,20},{20,24},{24,28},{1,5},{5,9},{9,... | collective-permute-start | bytes 98312 | tf_op jit(solution)/shard_map/ppermute | solution.py:16
  79.9 80.3 %all-gather.8.cloned.1.call-start = ((), (), s32[]{:S(2)}) async-start(), calls=%async_computation.11 | async-start | bytes 5242880 | tf_op jit(solution)/shard_map/all_gather | solution.py:121
  108.6 82.6 %all-gather.10.cloned.1.call-start = ((), (), s32[]{:S(2)}) async-start(), calls=%async_computation.12 | async-start | bytes 5242880 | tf_op jit(solution)/shard_map/all_gather | solution.py:121
  138.1 4.3 %copy-start.13 = (bf16[512,4096]{1,0:T(8,128)(2,1)S(1)}, bf16[512,4096]{1,0:T(8,128)(2,1)}, u32[]{:S(2)}) copy-start(bf16[512,4096]{1,0:T(8,128)(2,1)} %all-gather.6.cloned.1.call-done) | copy-start | bytes 12582916
  138.1 4.8 %copy-start.14 = (bf16[1,4096,256]{2,1,0:T(8,128)(2,1)S(1)}, bf16[1,4096,256]{2,1,0:T(8,128)(2,1)}, u32[]{:S(2)}) copy-start(bf16[1,4096,256]{2,1,0:T(8,128)(2,1)} %param.20) | copy-start | bytes 6291460
  145.0 9.4 %all-to-all-start.2 = ((bf16[4,128,256]{2,1,0:T(8,128)(2,1)}), bf16[4,128,256]{2,1,0:T(8,128)(2,1)S(1)}, u32[]{:S(2)}, u32[]{:S(2)}) async-start(bf16[4,128,256]{2,1,0:T(8,128)(2,1)} %pad_maximum_fusion), calls=%async_computation.2 | async-start | bytes 524288 | tf_op jit(solution)/shard_map/all_to_all | solution.py:131
  160.2 4.9 %copy-start.12 = (bf16[512,4096]{1,0:T(8,128)(2,1)S(1)}, bf16[512,4096]{1,0:T(8,128)(2,1)}, u32[]{:S(2)}) copy-start(bf16[512,4096]{1,0:T(8,128)(2,1)} %all-gather.8.cloned.1.call-done) | copy-start | bytes 12582916
  160.2 5.4 %copy-start.15 = (bf16[1,4096,256]{2,1,0:T(8,128)(2,1)S(1)}, bf16[1,4096,256]{2,1,0:T(8,128)(2,1)}, u32[]{:S(2)}) copy-start(bf16[1,4096,256]{2,1,0:T(8,128)(2,1)} %param.20) | copy-start | bytes 6291460
  167.6 12.6 %all-to-all-start.5 = ((bf16[4,128,256]{2,1,0:T(8,128)(2,1)}), bf16[4,128,256]{2,1,0:T(8,128)(2,1)S(1)}, u32[]{:S(2)}, u32[]{:S(2)}) async-start(bf16[4,128,256]{2,1,0:T(8,128)(2,1)} %pad_maximum_fusion.1), calls=%async_computation.5 | async-start | bytes 524288 | tf_op jit(solution)/shard_map/all_to_all | solution.py:131
  180.3 4.1 %copy-start.6 = (bf16[4,128,256]{2,1,0:T(8,128)(2,1)}, bf16[4,128,256]{2,1,0:T(8,128)(2,1)S(1)}, u32[]{:S(2)}) copy-start(bf16[4,128,256]{2,1,0:T(8,128)(2,1)S(1)} %all-to-all-done.5) | copy-start | bytes 786436
  180.3 29.8 %all-to-all-start.4 = ((bf16[8,16,4096]{2,1,0:T(8,128)(2,1)}), bf16[8,16,4096]{2,1,0:T(8,128)(2,1)S(1)}, u32[]{:S(2)}, u32[]{:S(2)}) async-start(bf16[8,16,4096]{2,1,0:T(8,128)(2,1)} %bitcast.138), calls=%async_computation.4 | async-start | bytes 2097152 | tf_op jit(solution)/shard_map/all_to_all | solution.py:138
  191.2 4.3 %copy-start.11 = (bf16[512,4096]{1,0:T(8,128)(2,1)S(1)}, bf16[512,4096]{1,0:T(8,128)(2,1)}, u32[]{:S(2)}) copy-start(bf16[512,4096]{1,0:T(8,128)(2,1)} %all-gather.10.cloned.1.call-done) | copy-start | bytes 12582916
  191.2 4.7 %copy-start.16 = (bf16[1,4096,256]{2,1,0:T(8,128)(2,1)S(1)}, bf16[1,4096,256]{2,1,0:T(8,128)(2,1)}, u32[]{:S(2)}) copy-start(bf16[1,4096,256]{2,1,0:T(8,128)(2,1)} %param.20) | copy-start | bytes 6291460
  210.1 9.4 %all-to-all-start.8 = ((bf16[4,128,256]{2,1,0:T(8,128)(2,1)}), bf16[4,128,256]{2,1,0:T(8,128)(2,1)S(1)}, u32[]{:S(2)}, u32[]{:S(2)}) async-start(bf16[4,128,256]{2,1,0:T(8,128)(2,1)} %pad_maximum_fusion.2), calls=%async_computation.8 | async-start | bytes 524288 | tf_op jit(solution)/shard_map/all_to_all | solution.py:131
  219.5 7.1 %copy-start.5 = (bf16[4,128,256]{2,1,0:T(8,128)(2,1)}, bf16[4,128,256]{2,1,0:T(8,128)(2,1)S(1)}, u32[]{:S(2)}) copy-start(bf16[4,128,256]{2,1,0:T(8,128)(2,1)S(1)} %all-to-all-done.8) | copy-start | bytes 786436
  219.5 30.0 %all-to-all-start.6 = ((bf16[8,16,4096]{2,1,0:T(8,128)(2,1)}), bf16[8,16,4096]{2,1,0:T(8,128)(2,1)}, u32[]{:S(2)}, u32[]{:S(2)}) async-start(bf16[8,16,4096]{2,1,0:T(8,128)(2,1)} %bitcast.139), calls=%async_computation.6 | async-start | bytes 2097152 | tf_op jit(solution)/shard_map/all_to_all | solution.py:138
  226.6 1.4 copy-start.1
  227.9 1.3 copy-start.2
  229.7 2.7 copy-start.3
  239.2 14.6 %copy-start.17 = (f32[1,1024]{1,0:T(1,128)S(1)}, f32[1,1024]{1,0:T(1,128)}, u32[]{:S(2)}) copy-start(f32[1,1024]{1,0:T(1,128)} %param.14) | copy-start | bytes 12292
  249.5 29.8 %all-to-all-start.9 = ((bf16[8,16,4096]{2,1,0:T(8,128)(2,1)}), bf16[8,16,4096]{2,1,0:T(8,128)(2,1)}, u32[]{:S(2)}, u32[]{:S(2)}) async-start(bf16[8,16,4096]{2,1,0:T(8,128)(2,1)} %bitcast.140), calls=%async_computation.9 | async-start | bytes 2097152 | tf_op jit(solution)/shard_map/all_to_all | solution.py:138
  261.8 0.8 copy-start.7
Sparse Core Ops, SparseCore 0:
  9.5 68.1 all-gather.11
  80.0 34.9 all-gather.5
  116.5 34.4 all-gather.7
  152.5 37.2 all-gather.9
